TPU v7x, 32 devices: a whole 2x2x4 slice. The times are simulated.
32 devices in a mesh: ep: 4 (over y, x), tp: 8 (over z, core).
Axes of the slice: x: 2, y: 2, z: 4, core: 2. Of those that a mesh axis runs over, the one named last changes fastest.
Arguments:
- features: bfloat16 [64, 1024], P('ep', 'tp'), may hold values from -6 to 6
- key_table: bfloat16 [65536, 1024], P('ep', 'tp'), may hold values from -0.1875 to 0.1875
- value_table: bfloat16 [65536, 1024], P('ep', 'tp'), may hold values from -6 to 6
- chosen: int32 [64, 4, 16], P('ep'), may hold values from 0 to 65535
- scores: float32 [64, 4, 16], P('ep'), may hold values from -8 to 8
Outputs:
- mixed: bfloat16 [64, 1024], P('ep', 'tp')
Inputs may be any that keep to these rules, and one draw needn't show every extreme that they name: Every chosen row is a row of the tables, 0 to 65535; rows may repeat, and a few rows are far more popular than the rest.
All inputs are finite; a program needn't handle non-finite values.
Results may differ from a plain program's by a relative error of at most 0.0065.
Values may be sent and summed in bfloat16 or wider, within the bound.
A program may use at most 64 MiB of HBM per device.

v0:
```python
import jax
import jax.numpy as jnp
from jax import lax
from jax.sharding import PartitionSpec as P


def in_blocks(func, arrays):
    total = arrays[0].shape[0]
    width = 32 if total % 32 == 0 else total
    count = total // width
    if count == 1:
        return func(arrays)
    shaped = tuple((item.reshape((count, width) + item.shape[1:]) for item in arrays))
    result = lax.map(func, shaped)
    return result.reshape((total,) + result.shape[2:])


def shards(features, key_table, value_table, chosen, scores):
    table_rows = key_table.shape[0]
    head_count = chosen.shape[1]
    top_count = chosen.shape[2]
    first_row = lax.axis_index("ep") * table_rows
    gate_weights = jax.nn.softmax(scores, axis=-1)
    chosen_all = lax.all_gather(chosen, "ep", axis=0, tiled=True)
    gates_all = lax.all_gather(gate_weights, "ep", axis=0, tiled=True)
    shifted = chosen_all - first_row
    owned_mask = (shifted >= 0) & (shifted < table_rows)
    local_rows = jnp.clip(shifted, 0, table_rows - 1).reshape(shifted.shape[0], -1)

    def dots_block(pair):
        token_block, picked = pair
        dense = lax.dot_general(
            token_block, key_table, (((1,), (1,)), ((), ())), preferred_element_type=jnp.float32
        )
        return jnp.take_along_axis(dense, picked, axis=1)

    def partial_dots(token_block):
        row_count = token_block.shape[0]
        picked = lax.slice_in_dim(local_rows, 0, row_count, axis=0)
        keep_mask = lax.slice_in_dim(owned_mask, 0, row_count, axis=0)
        products = in_blocks(dots_block, (token_block, picked))
        return jnp.where(keep_mask.reshape(row_count, -1), products, 0.0)

    partial_value = partial_dots(lax.all_gather(features, "ep", axis=0, tiled=True))
    partial_value = partial_value.reshape(-1, head_count, top_count)
    products = lax.psum(partial_value, "tp")
    row_weights = (gates_all * jax.nn.gelu(products, approximate=False)).astype(jnp.bfloat16)
    row_weights = jnp.where(owned_mask, row_weights, jnp.zeros_like(row_weights))
    flat_weights = row_weights.reshape(row_weights.shape[0], -1)

    def value_block(pair):
        block_weights, picked = pair
        width = picked.shape[0]
        token_ids = lax.broadcasted_iota(jnp.int32, picked.shape, 0)
        dense = (
            jnp.zeros((width, table_rows), jnp.float32)
            .at[token_ids, picked]
            .add(block_weights.astype(jnp.float32))
        )
        upper = dense.astype(jnp.bfloat16)
        lower = (dense - upper.astype(jnp.float32)).astype(jnp.bfloat16)
        summed = jnp.dot(upper, value_table, preferred_element_type=jnp.float32)
        return summed + jnp.dot(lower, value_table, preferred_element_type=jnp.float32)

    def owner_term(row_count):
        picked = lax.slice_in_dim(local_rows, 0, row_count, axis=0)
        block_weights = lax.slice_in_dim(flat_weights, 0, row_count, axis=0)
        return in_blocks(value_block, (block_weights, picked))

    summed = lax.psum_scatter(
        owner_term(lax.axis_size("ep") * features.shape[0]), "ep", scatter_dimension=0, tiled=True
    )
    return summed.astype(jnp.bfloat16)


def solution(mesh):
    return jax.shard_map(
        shards,
        mesh=mesh,
        in_specs=(
            P("ep", "tp"),
            P("ep", "tp"),
            P("ep", "tp"),
            P("ep", None, None),
            P("ep", None, None),
        ),
        out_specs=P("ep", "tp"),
        check_vma=False,
    )
```

profile of v0, /device:TPU:0, one launch (start us, length us, event | category | flops | bytes accessed | tf_op | source)
XLA Modules:
  0.0 150.6 jit_solution(2925781054300284029)
XLA Ops:
  0.0 10.1 %all_gather.9 = s32[64,4,16]{2,1,0:T(4,128)S(1)} all-gather(s32[16,4,16]{2,1,0:T(4,128)} %param.12), channel_id=1, replica_groups=mesh['ep'=4,'tp'=8] {'ep'}, dimensions={0}, use_global_device_ids=true | all-gather | bytes 20480 | tf_op jit(solution)/shard_map/all_gather | solution.py:24
  10.1 0.1 copy.12
  10.2 0.1 reshape_reshape.7
  10.3 0.1 copy.16
  10.4 8.0 %all_gather.11 = bf16[64,128]{1,0:T(8,128)(2,1)S(1)} all-gather(bf16[16,128]{1,0:T(8,128)(2,1)} %param.9), channel_id=1, replica_groups=mesh['ep'=4,'tp'=8] {'ep'}, dimensions={0}, use_global_device_ids=true | all-gather | bytes 20480 | tf_op jit(solution)/shard_map/all_gather | solution.py:44
  18.4 0.0 copy-start.3
  18.4 0.0 copy-start.1
  18.4 0.0 copy-start.2
  18.4 41.2 %while.20 = (s32[]{:T(128)}, f32[2,32,64]{2,1,0:T(8,128)S(1)}, s32[2,32,64]{2,1,0:T(8,128)S(1)}, bf16[2,32,128]{2,1,0:T(8,128)(2,1)S(1)}, bf16[16384,128]{1,0:T(8,128)(2,1)}, /*index=5*/s32[]{:T(128)}) while((s32[]{:T(128)}, f32[2,32,64]{2,1,0:T(8,128)S(1)}, s32[2,32,64]{2,1,0:T(8,128)S(1)}, bf16[2,32,128]{2,1,0:T(8,128)(2,1)S(1)}, ...), condition=%wide.region_3.4_spmd, body=%wide.region_2.3_spmd.sunk | while | flops 134248448 | bytes 6430801 | solution.py:14
  18.4 3.7 %fusion.47 = f32[32,16384]{1,0:T(8,128)S(1)} fusion(bf16[16384,128]{1,0:T(8,128)(2,1)} %get-tuple-element.181, bf16[2,32,128]{2,1,0:T(8,128)(2,1)S(1)} %get-tuple-element.180, s32[]{:T(128)} %get-tuple-element.171), kind=kOutput, calls=%fused_computation.8.clone.1 | convolution fusion | flops 134217728 | bytes 6299652 | tf_op jit(solution)/shard_map/while/body/eval_jaxpr/dot_general | solution.py:32
  22.2 0.1 reshape.128
  22.2 16.6 %gather_fusion = f32[2048]{0:T(1024)S(1)} fusion(f32[32,16384]{1,0:T(8,128)S(1)} %fusion.47, s32[2048]{0:T(1024)S(1)} %reshape.128), kind=kCustom, calls=%fused_computation.clone.1 | custom fusion | bytes 32768 | tf_op jit(solution)/shard_map/while/body/eval_jaxpr/jit(take_along_axis)/gather | solution.py:35
  38.9 0.1 gather.11
  39.0 3.7 %fusion.47 = f32[32,16384]{1,0:T(8,128)S(1)} fusion(bf16[16384,128]{1,0:T(8,128)(2,1)} %get-tuple-element.181, bf16[2,32,128]{2,1,0:T(8,128)(2,1)S(1)} %get-tuple-element.180, s32[]{:T(128)} %get-tuple-element.171), kind=kOutput, calls=%fused_computation.8.clone.1 | convolution fusion | flops 134217728 | bytes 6299652 | tf_op jit(solution)/shard_map/while/body/eval_jaxpr/dot_general | solution.py:32
  42.7 0.1 reshape.128
  42.8 16.6 %gather_fusion = f32[2048]{0:T(1024)S(1)} fusion(f32[32,16384]{1,0:T(8,128)S(1)} %fusion.47, s32[2048]{0:T(1024)S(1)} %reshape.128), kind=kCustom, calls=%fused_computation.clone.1 | custom fusion | bytes 32768 | tf_op jit(solution)/shard_map/while/body/eval_jaxpr/jit(take_along_axis)/gather | solution.py:35
  59.5 0.1 gather.11
  59.6 0.1 copy.14
  59.6 0.1 reshape.94
  59.8 26.0 %psum.7 = f32[64,4,16]{0,2,1:T(8,128)S(1)} all-reduce(f32[64,4,16]{0,2,1:T(8,128)S(1)} %get-tuple-element.101), channel_id=1, replica_groups=mesh['ep'=4,'tp'=8] {'tp'}, use_global_device_ids=true, to_apply=%region_4.5 | all-reduce | flops 4096 | bytes 32768 | tf_op jit(solution)/shard_map/psum | solution.py:46
  85.8 0.0 copy-done.3
  85.8 0.2 fusion.17
  86.0 7.7 %all_gather.10 = f32[64,4,16]{2,1,0:T(4,128)S(1)} all-gather(f32[16,4,16]{2,1,0:T(4,128)S(1)} %fusion.17), channel_id=1, replica_groups=mesh['ep'=4,'tp'=8] {'ep'}, dimensions={0}, use_global_device_ids=true | all-gather | bytes 20480 | tf_op jit(solution)/shard_map/all_gather | solution.py:25
  93.6 0.1 copy.15
  93.7 0.1 fusion.30
  93.8 0.1 reshape_reshape.8
  93.9 0.1 copy.17
  94.0 0.0 copy-done.1
  94.0 0.0 copy-done.2
  94.0 0.0 copy-start.4
  94.0 39.5 %while.21 = (s32[]{:T(128)}, f32[2,32,128]{2,1,0:T(8,128)S(1)}, s32[2,32,64]{2,1,0:T(8,128)S(1)}, bf16[2,32,64]{2,1,0:T(8,128)(2,1)S(1)}, bf16[16384,128]{1,0:T(...) while((s32[]{:T(128)}, f32[2,32,128]{2,1,0:T(8,128)S(1)}, ...), condition=%wide.region_7.8_spmd, body=%wide.region_5.7_spmd.sunk | while | flops 271101952 | bytes 35831960 | solution.py:14
  94.1 0.1 multiply_reduce_fusion.2
  94.1 0.1 and_reduce_fusion.2
  94.2 0.1 reshape.131
  94.3 0.1 reshape.132
  94.4 13.3 %scatter_custom_fusion.5 = f32[524288]{0:T(1024)} fusion(s32[2048]{0:T(1024)S(1)} %reshape.131, f32[2048]{0:T(1024)S(1)} %reshape.132, f32[]{:T(128)} %constant.53.clone.1..sunk), kind=kCustom, calls=%fused_computation.16.clone.1 | custom fusion | flops 2048 | bytes 2097156 | tf_op jit(solution)/shard_map/while
  107.7 1.7 %reshape.133 = f32[32,16384]{1,0:T(8,128)S(1)} reshape(f32[524288]{0:T(1024)} %scatter_custom_fusion.5) | data formatting | bytes 4194304 | tf_op jit(solution)/shard_map/while/body/eval_jaxpr/scatter-add | solution.py:58
  109.5 0.0 copy-start
  109.5 3.1 %fusion.53 = f32[32,128]{1,0:T(8,128)S(1)} fusion(bf16[16384,128]{1,0:T(8,128)(2,1)} %get-tuple-element.205, f32[32,16384]{1,0:T(8,128)S(1)} %reshape.133), kind=kOutput, calls=%fused_computation.19.clone.1 | convolution fusion | flops 134742016 | bytes 6307840 | tf_op jit(solution)/shard_map/while/body/eval_jaxpr/dot_general | solution.py:62
  112.6 0.3 copy-done
  112.9 0.8 fusion.54
  113.8 0.1 multiply_reduce_fusion.2
  113.8 0.1 and_reduce_fusion.2
  113.9 0.1 reshape.131
  114.0 0.1 reshape.132
  114.1 13.5 %scatter_custom_fusion.5 = f32[524288]{0:T(1024)} fusion(s32[2048]{0:T(1024)S(1)} %reshape.131, f32[2048]{0:T(1024)S(1)} %reshape.132, f32[]{:T(128)} %constant.53.clone.1..sunk), kind=kCustom, calls=%fused_computation.16.clone.1 | custom fusion | flops 2048 | bytes 2097156 | tf_op jit(solution)/shard_map/while
  127.6 1.7 %reshape.133 = f32[32,16384]{1,0:T(8,128)S(1)} reshape(f32[524288]{0:T(1024)} %scatter_custom_fusion.5) | data formatting | bytes 4194304 | tf_op jit(solution)/shard_map/while/body/eval_jaxpr/scatter-add | solution.py:58
  129.3 0.0 copy-start
  129.3 3.1 %fusion.53 = f32[32,128]{1,0:T(8,128)S(1)} fusion(bf16[16384,128]{1,0:T(8,128)(2,1)} %get-tuple-element.205, f32[32,16384]{1,0:T(8,128)S(1)} %reshape.133), kind=kOutput, calls=%fused_computation.19.clone.1 | convolution fusion | flops 134742016 | bytes 6307840 | tf_op jit(solution)/shard_map/while/body/eval_jaxpr/dot_general | solution.py:62
  132.4 0.3 copy-done
  132.8 0.8 fusion.54
  133.6 15.1 %all-reduce = bf16[64,128]{1,0:T(8,128)(2,1)S(1)} all-reduce(f32[64,128]{1,0:T(8,128)S(1)} %bitcast.41), channel_id=2, replica_groups=mesh['ep'=4,'tp'=8] {'ep'}, use_global_device_ids=true, to_apply=%region_8.9.clone | all-reduce | flops 8192 | bytes 49152
  148.7 0.0 copy-done.4
  148.7 0.6 dynamic-slice
  150.0 0.6 dynamic-slice_convert_fusion.1
  (16 shorter events, 0.2 us)
Async XLA Ops:
  18.4 67.4 %copy-start.3 = (f32[16,4,16]{2,1,0:T(4,128)S(1)}, f32[16,4,16]{2,1,0:T(4,128)}, u32[]{:S(2)}) copy-start(f32[16,4,16]{2,1,0:T(4,128)} %param.13) | copy-start | bytes 12292
  18.4 75.6 %copy-start.1 = (s32[2]{0:T(128)S(1)}, s32[2]{0:T(128)}, u32[]{:S(2)}) copy-start(s32[2]{0:T(128)} %constant.199) | copy-start | bytes 28
  18.4 75.6 %copy-start.2 = (s32[2]{0:T(128)S(1)}, s32[2]{0:T(128)}, u32[]{:S(2)}) copy-start(s32[2]{0:T(128)} %constant.200) | copy-start | bytes 28
  94.0 54.7 %copy-start.4 = (u32[32]{0:T(128)S(1)}, u32[32]{0:T(128)}, u32[]{:S(2)}) copy-start(u32[32]{0:T(128)} %constant.148) | copy-start | bytes 388
  109.5 3.5 %copy-start = (bf16[16384,128]{1,0:T(8,128)(2,1)S(1)}, bf16[16384,128]{1,0:T(8,128)(2,1)}, u32[]{:S(2)}) copy-start(bf16[16384,128]{1,0:T(8,128)(2,1)} %get-tuple-element.205) | copy-start | bytes 12582916 | tf_op jit(solution)/shard_map/while
  129.3 3.5 %copy-start = (bf16[16384,128]{1,0:T(8,128)(2,1)S(1)}, bf16[16384,128]{1,0:T(8,128)(2,1)}, u32[]{:S(2)}) copy-start(bf16[16384,128]{1,0:T(8,128)(2,1)} %get-tuple-element.205) | copy-start | bytes 12582916 | tf_op jit(solution)/shard_map/while
where the time goes:
time: 151 us
  blocking collectives  66.9 us (44%)
  local copies, waits for them, and re-layouts  40 us (26%)
  other arithmetic  27.6 us (18%)
  matrix products  15.2 us (10%)
    gather x6, local copies, waits for them, and re-layouts, dots_block(): return jnp.take_along_axis(dense, picked, axis=1)  33.6 us
    while x8, other arithmetic  27.1 us
    psum x1, blocking collectives, shards(): products = lax.psum(partial_value, 'tp')  26 us
    unnamed x1, blocking collectives  15.1 us
    all_gather x1, blocking collectives, shards(): chosen_all = lax.all_gather(chosen, 'ep', axis=0, tiled=True)  10.1 us
    all_gather x1, blocking collectives, shards(): lax.all_gather(features, 'ep', axis=0, tiled=True)  7.96 us
    all_gather x1, blocking collectives, shards(): gates_all = lax.all_gather(gate_weights, 'ep', axis=0, tiled=True)  7.69 us
    dot_general x2, matrix products, dots_block(): lax.dot_general(token_block, key_table, (((1,), (1,)), ((), ())), preferr...  7.45 us

commit v1 on v0

--- a/solution.py
+++ b/solution.py
@@ -2,6 +2,7 @@
 import jax.numpy as jnp
 from jax import lax
 from jax.sharding import PartitionSpec as P
+from jax.lax import axis_size, ppermute
 
 
 def in_blocks(func, arrays):
@@ -43,7 +44,26 @@
 
     partial_value = partial_dots(lax.all_gather(features, "ep", axis=0, tiled=True))
     partial_value = partial_value.reshape(-1, head_count, top_count)
-    products = lax.psum(partial_value, "tp")
+
+    def draw_the_matrix(original, named_axis):
+        num = axis_size(named_axis)
+
+        def press_modes(newest, v_now):
+            if v_now >= num:
+                return newest
+            new = press_modes(
+                newest
+                + ppermute(
+                    newest, named_axis, tuple(((src_i, src_i ^ v_now) for src_i in range(num)))
+                ),
+                2 * v_now,
+            )
+            return new
+
+        block_next = press_modes(original, 1)
+        return block_next
+
+    products = draw_the_matrix(partial_value, named_axis="tp")
     row_weights = (gates_all * jax.nn.gelu(products, approximate=False)).astype(jnp.bfloat16)
     row_weights = jnp.where(owned_mask, row_weights, jnp.zeros_like(row_weights))
     flat_weights = row_weights.reshape(row_weights.shape[0], -1)

time: 151 us -> 133 us (0.88)
  blocking collectives: 66.9 us -> 41.2 us
  starting transfers between devices: 0 us -> 4.23 us
  waiting for transfers between devices: 0 us -> 3.54 us
    psum x1 -> x0, blocking collectives: 26 us -> none  [shards(): products = lax.psum(partial_value, 'tp')]
    ppermute x0 -> x3, starting transfers between devices: none -> 4.23 us  [press_modes(): ppermute(newest, named_axis, tuple(((src_i, src_i ^ v_now) for src_i in r...]
    ppermute x0 -> x3, waiting for transfers between devices: none -> 3.54 us  [press_modes(): ppermute(newest, named_axis, tuple(((src_i, src_i ^ v_now) for src_i in r...]
  transfers between devices with their start and end apart: 0 -> 3, of which waited for: 0 -> 2; matrix products, arithmetic and copies ran while one was open for 0% -> 1% of each run, Pallas kernels for 0% -> 0%
where the time goes in v1:
time: 133 us
  blocking collectives  41.2 us (31%)
  local copies, waits for them, and re-layouts  40.1 us (30%)
  other arithmetic  27.6 us (21%)
  matrix products  15.2 us (11%)
  starting transfers between devices  4.23 us (3%)
  waiting for transfers between devices  3.54 us (3%)
    gather x6, local copies, waits for them, and re-layouts, dots_block(): return jnp.take_along_axis(dense, picked, axis=1)  33.6 us
    while x8, other arithmetic  27.1 us
    unnamed x1, blocking collectives  15.2 us
    all_gather x1, blocking collectives, shards(): chosen_all = lax.all_gather(chosen, 'ep', axis=0, tiled=True)  10.1 us
    all_gather x1, blocking collectives, shards(): lax.all_gather(features, 'ep', axis=0, tiled=True)  7.96 us
    all_gather x1, blocking collectives, shards(): gates_all = lax.all_gather(gate_weights, 'ep', axis=0, tiled=True)  7.86 us
    dot_general x2, matrix products, dots_block(): lax.dot_general(token_block, key_table, (((1,), (1,)), ((), ())), preferr...  7.46 us
    dot_general x2, matrix products, value_block(): summed = jnp.dot(upper, value_table, preferred_element_type=jnp.float32)  6.18 us
  transfers between devices with their start and end apart: 3, of which 2 were waited for; matrix products, arithmetic and copies ran while one was open for 1% of the time, Pallas kernels for 0%

profile of v1, /device:TPU:0, one launch (start us, length us, event | category | flops | bytes accessed | tf_op | source)
XLA Modules:
  0.0 132.8 jit_solution(15712404637451524408)
XLA Ops:
  0.0 10.1 %all_gather.9 = s32[64,4,16]{2,1,0:T(4,128)S(1)} all-gather(s32[16,4,16]{2,1,0:T(4,128)} %param.12), channel_id=1, replica_groups=mesh['ep'=4,'tp'=8] {'ep'}, dimensions={0}, use_global_device_ids=true | all-gather | bytes 20480 | tf_op jit(solution)/shard_map/all_gather | solution.py:25
  10.1 0.1 copy.12
  10.2 0.1 reshape_reshape.7
  10.3 0.1 copy.16
  10.4 8.0 %all_gather.11 = bf16[64,128]{1,0:T(8,128)(2,1)S(1)} all-gather(bf16[16,128]{1,0:T(8,128)(2,1)} %param.9), channel_id=1, replica_groups=mesh['ep'=4,'tp'=8] {'ep'}, dimensions={0}, use_global_device_ids=true | all-gather | bytes 20480 | tf_op jit(solution)/shard_map/all_gather | solution.py:45
  18.4 0.0 copy-start.3
  18.4 0.0 copy-start.4
  18.4 0.0 copy-start.1
  18.4 0.0 copy-start.2
  18.4 41.2 %while.20 = (s32[]{:T(128)}, f32[2,32,64]{2,1,0:T(8,128)S(1)}, s32[2,32,64]{2,1,0:T(8,128)S(1)}, bf16[2,32,128]{2,1,0:T(8,128)(2,1)S(1)}, bf16[16384,128]{1,0:T(8,128)(2,1)}, /*index=5*/s32[]{:T(128)}) while((s32[]{:T(128)}, f32[2,32,64]{2,1,0:T(8,128)S(1)}, s32[2,32,64]{2,1,0:T(8,128)S(1)}, bf16[2,32,128]{2,1,0:T(8,128)(2,1)S(1)}, ...), condition=%wide.region_3.4_spmd, body=%wide.region_2.3_spmd.sunk | while | flops 134248448 | bytes 6430801 | solution.py:15
  18.4 3.7 %fusion.47 = f32[32,16384]{1,0:T(8,128)S(1)} fusion(bf16[16384,128]{1,0:T(8,128)(2,1)} %get-tuple-element.181, bf16[2,32,128]{2,1,0:T(8,128)(2,1)S(1)} %get-tuple-element.180, s32[]{:T(128)} %get-tuple-element.171), kind=kOutput, calls=%fused_computation.8.clone.1 | convolution fusion | flops 134217728 | bytes 6299652 | tf_op jit(solution)/shard_map/while/body/eval_jaxpr/dot_general | solution.py:33
  22.2 0.1 reshape.128
  22.3 16.6 %gather_fusion = f32[2048]{0:T(1024)S(1)} fusion(f32[32,16384]{1,0:T(8,128)S(1)} %fusion.47, s32[2048]{0:T(1024)S(1)} %reshape.128), kind=kCustom, calls=%fused_computation.clone.1 | custom fusion | bytes 32768 | tf_op jit(solution)/shard_map/while/body/eval_jaxpr/jit(take_along_axis)/gather | solution.py:36
  38.9 0.1 gather.11
  39.0 3.7 %fusion.47 = f32[32,16384]{1,0:T(8,128)S(1)} fusion(bf16[16384,128]{1,0:T(8,128)(2,1)} %get-tuple-element.181, bf16[2,32,128]{2,1,0:T(8,128)(2,1)S(1)} %get-tuple-element.180, s32[]{:T(128)} %get-tuple-element.171), kind=kOutput, calls=%fused_computation.8.clone.1 | convolution fusion | flops 134217728 | bytes 6299652 | tf_op jit(solution)/shard_map/while/body/eval_jaxpr/dot_general | solution.py:33
  42.8 0.1 reshape.128
  42.8 16.6 %gather_fusion = f32[2048]{0:T(1024)S(1)} fusion(f32[32,16384]{1,0:T(8,128)S(1)} %fusion.47, s32[2048]{0:T(1024)S(1)} %reshape.128), kind=kCustom, calls=%fused_computation.clone.1 | custom fusion | bytes 32768 | tf_op jit(solution)/shard_map/while/body/eval_jaxpr/jit(take_along_axis)/gather | solution.py:36
  59.5 0.1 gather.11
  59.6 0.1 copy.14
  59.7 0.1 reshape.94
  59.8 0.1 collective-permute-start
  59.9 1.2 collective-permute-done
  61.1 1.6 %collective-permute-start.1 = (f32[64,4,16]{0,2,1:T(8,128)S(1)}, f32[64,4,16]{0,2,1:T(8,128)S(1)}, u32[]{:S(2)}, u32[]{:S(2)}) collective-permute-start(f32[64,4,16]{0,2,1:T(8,128)S(1)} %add.56), channel_id=1, source_target_pairs={{0,2},{1,3},{2,0},{3,1},{4,6},{5,7},{6,4},{7,5},{8,10},{9,11},{10,... | collective-permute-start | bytes 49160 | tf_op jit(solution)/shard_map/ppermute | solution.py:56
  62.6 2.3 %collective-permute-done.1 = f32[64,4,16]{0,2,1:T(8,128)S(1)} collective-permute-done((f32[64,4,16]{0,2,1:T(8,128)S(1)}, f32[64,4,16]{0,2,1:T(8,128)S(1)}, u32[]{:S(2)}, u32[]{:S(2)}) %collective-permute-start.1) | collective-permute-done | bytes 16416 | tf_op jit(solution)/shard_map/ppermute | solution.py:56
  65.0 2.6 %collective-permute-start.2 = (f32[64,4,16]{0,2,1:T(8,128)S(1)}, f32[64,4,16]{0,2,1:T(8,128)S(1)}, u32[]{:S(2)}, u32[]{:S(2)}) collective-permute-start(f32[64,4,16]{0,2,1:T(8,128)S(1)} %add.57), channel_id=1, source_target_pairs={{0,4},{1,5},{2,6},{3,7},{4,0},{5,1},{6,2},{7,3},{8,12},{9,13},{10,... | collective-permute-start | bytes 49160 | tf_op jit(solution)/shard_map/ppermute | solution.py:56
  67.6 0.0 copy-done.3
  67.6 0.2 fusion.17
  67.8 7.9 %all_gather.10 = f32[64,4,16]{2,1,0:T(4,128)S(1)} all-gather(f32[16,4,16]{2,1,0:T(4,128)S(1)} %fusion.17), channel_id=1, replica_groups=mesh['ep'=4,'tp'=8] {'ep'}, dimensions={0}, use_global_device_ids=true | all-gather | bytes 20480 | tf_op jit(solution)/shard_map/all_gather | solution.py:26
  75.6 0.1 copy.15
  75.7 0.0 copy-done.4
  75.7 0.7 dynamic-slice
  77.1 0.0 collective-permute-done.2
  77.1 0.1 fusion.30
  77.2 0.1 reshape_reshape.8
  77.3 0.1 copy.17
  77.4 0.0 copy-done.1
  77.4 0.0 copy-done.2
  77.4 39.5 %while.21 = (s32[]{:T(128)}, f32[2,32,128]{2,1,0:T(8,128)S(1)}, s32[2,32,64]{2,1,0:T(8,128)S(1)}, bf16[2,32,64]{2,1,0:T(8,128)(2,1)S(1)}, bf16[16384,128]{1,0:T(...) while((s32[]{:T(128)}, f32[2,32,128]{2,1,0:T(8,128)S(1)}, ...), condition=%wide.region_6.7_spmd, body=%wide.region_4.6_spmd.sunk | while | flops 271101952 | bytes 35831960 | solution.py:15
  77.4 0.1 multiply_reduce_fusion.2
  77.5 0.1 and_reduce_fusion.2
  77.6 0.1 reshape.131
  77.7 0.1 reshape.132
  77.8 13.3 %scatter_custom_fusion.5 = f32[524288]{0:T(1024)} fusion(s32[2048]{0:T(1024)S(1)} %reshape.131, f32[2048]{0:T(1024)S(1)} %reshape.132, f32[]{:T(128)} %constant.53.clone.1..sunk), kind=kCustom, calls=%fused_computation.16.clone.1 | custom fusion | flops 2048 | bytes 2097156 | tf_op jit(solution)/shard_map/while
  91.1 1.7 %reshape.133 = f32[32,16384]{1,0:T(8,128)S(1)} reshape(f32[524288]{0:T(1024)} %scatter_custom_fusion.5) | data formatting | bytes 4194304 | tf_op jit(solution)/shard_map/while/body/eval_jaxpr/scatter-add | solution.py:78
  92.8 0.0 copy-start
  92.9 3.1 %fusion.53 = f32[32,128]{1,0:T(8,128)S(1)} fusion(bf16[16384,128]{1,0:T(8,128)(2,1)} %get-tuple-element.205, f32[32,16384]{1,0:T(8,128)S(1)} %reshape.133), kind=kOutput, calls=%fused_computation.19.clone.1 | convolution fusion | flops 134742016 | bytes 6307840 | tf_op jit(solution)/shard_map/while/body/eval_jaxpr/dot_general | solution.py:82
  95.9 0.3 copy-done
  96.3 0.8 fusion.54
  97.1 0.1 multiply_reduce_fusion.2
  97.2 0.1 and_reduce_fusion.2
  97.3 0.1 reshape.131
  97.4 0.1 reshape.132
  97.4 13.5 %scatter_custom_fusion.5 = f32[524288]{0:T(1024)} fusion(s32[2048]{0:T(1024)S(1)} %reshape.131, f32[2048]{0:T(1024)S(1)} %reshape.132, f32[]{:T(128)} %constant.53.clone.1..sunk), kind=kCustom, calls=%fused_computation.16.clone.1 | custom fusion | flops 2048 | bytes 2097156 | tf_op jit(solution)/shard_map/while
  110.9 1.7 %reshape.133 = f32[32,16384]{1,0:T(8,128)S(1)} reshape(f32[524288]{0:T(1024)} %scatter_custom_fusion.5) | data formatting | bytes 4194304 | tf_op jit(solution)/shard_map/while/body/eval_jaxpr/scatter-add | solution.py:78
  112.7 0.0 copy-start
  112.7 3.1 %fusion.53 = f32[32,128]{1,0:T(8,128)S(1)} fusion(bf16[16384,128]{1,0:T(8,128)(2,1)} %get-tuple-element.205, f32[32,16384]{1,0:T(8,128)S(1)} %reshape.133), kind=kOutput, calls=%fused_computation.19.clone.1 | convolution fusion | flops 134742016 | bytes 6307840 | tf_op jit(solution)/shard_map/while/body/eval_jaxpr/dot_general | solution.py:82
  115.8 0.3 copy-done
  116.1 0.8 fusion.54
  116.9 15.2 %all-reduce = bf16[64,128]{1,0:T(8,128)(2,1)S(1)} all-reduce(f32[64,128]{1,0:T(8,128)S(1)} %bitcast.41), channel_id=2, replica_groups=mesh['ep'=4,'tp'=8] {'ep'}, use_global_device_ids=true, to_apply=%region_7.8.clone | all-reduce | flops 8192 | bytes 49152
  132.2 0.6 dynamic-slice_convert_fusion.1
  (18 shorter events, 0.2 us)
Async XLA Ops:
  18.4 49.2 %copy-start.3 = (f32[16,4,16]{2,1,0:T(4,128)S(1)}, f32[16,4,16]{2,1,0:T(4,128)}, u32[]{:S(2)}) copy-start(f32[16,4,16]{2,1,0:T(4,128)} %param.13) | copy-start | bytes 12292
  18.4 57.3 %copy-start.4 = (u32[32]{0:T(128)S(1)}, u32[32]{0:T(128)}, u32[]{:S(2)}) copy-start(u32[32]{0:T(128)} %constant.148) | copy-start | bytes 388
  18.4 59.0 %copy-start.1 = (s32[2]{0:T(128)S(1)}, s32[2]{0:T(128)}, u32[]{:S(2)}) copy-start(s32[2]{0:T(128)} %constant.199) | copy-start | bytes 28
  18.4 59.0 %copy-start.2 = (s32[2]{0:T(128)S(1)}, s32[2]{0:T(128)}, u32[]{:S(2)}) copy-start(s32[2]{0:T(128)} %constant.200) | copy-start | bytes 28
  59.8 1.3 collective-permute-start
  61.1 3.9 %collective-permute-start.1 = (f32[64,4,16]{0,2,1:T(8,128)S(1)}, f32[64,4,16]{0,2,1:T(8,128)S(1)}, u32[]{:S(2)}, u32[]{:S(2)}) collective-permute-start(f32[64,4,16]{0,2,1:T(8,128)S(1)} %add.56), channel_id=1, source_target_pairs={{0,2},{1,3},{2,0},{3,1},{4,6},{5,7},{6,4},{7,5},{8,10},{9,11},{10,... | collective-permute-start | bytes 49160 | tf_op jit(solution)/shard_map/ppermute | solution.py:56
  65.0 12.1 %collective-permute-start.2 = (f32[64,4,16]{0,2,1:T(8,128)S(1)}, f32[64,4,16]{0,2,1:T(8,128)S(1)}, u32[]{:S(2)}, u32[]{:S(2)}) collective-permute-start(f32[64,4,16]{0,2,1:T(8,128)S(1)} %add.57), channel_id=1, source_target_pairs={{0,4},{1,5},{2,6},{3,7},{4,0},{5,1},{6,2},{7,3},{8,12},{9,13},{10,... | collective-permute-start | bytes 49160 | tf_op jit(solution)/shard_map/ppermute | solution.py:56
  92.8 3.5 %copy-start = (bf16[16384,128]{1,0:T(8,128)(2,1)S(1)}, bf16[16384,128]{1,0:T(8,128)(2,1)}, u32[]{:S(2)}) copy-start(bf16[16384,128]{1,0:T(8,128)(2,1)} %get-tuple-element.205) | copy-start | bytes 12582916 | tf_op jit(solution)/shard_map/while
  112.7 3.5 %copy-start = (bf16[16384,128]{1,0:T(8,128)(2,1)S(1)}, bf16[16384,128]{1,0:T(8,128)(2,1)}, u32[]{:S(2)}) copy-start(bf16[16384,128]{1,0:T(8,128)(2,1)} %get-tuple-element.205) | copy-start | bytes 12582916 | tf_op jit(solution)/shard_map/while
